TPU v7x, 32 devices: a whole 2x2x4 slice. The times are simulated.
32 devices in a mesh: sp: 8 (over z, x), tp: 4 (over y, core).
Axes of the slice: x: 2, y: 2, z: 4, core: 2. Of those that a mesh axis runs over, the one named last changes fastest.
Arguments:
- latents: bfloat16 [4096, 2048], P(('sp', 'tp')), may hold values from -6 to 6
- context: bfloat16 [512, 2048], P('sp'), may hold values from -6 to 6
- cond: float32 [2048], P('sp'), may hold values from -6 to 6
- ctx_cond: float32 [2048], P('sp'), may hold values from -6 to 6
- mod_weight: float32 [2048, 6144], P('sp', 'tp'), may hold values from -0.125 to 0.125
- query_weight: bfloat16 [2048, 2048], P(None, 'tp'), may hold values from -1 to 1, as said below
- key_matrix: bfloat16 [2048, 1024], P(None, 'tp'), may hold values from -1 to 1, as said below
- value_matrix: bfloat16 [2048, 1024], P(None, 'tp'), may hold values from -0.125 to 0.125
- out_weight: bfloat16 [2048, 2048], P('tp'), may hold values from -0.125 to 0.125
- query_gain: float32 [128], replicated, may hold values from 0.7 to 7
- key_gain: float32 [128], replicated, may hold values from 0.7 to 7
Outputs:
- updated: bfloat16 [4096, 2048], P(('sp', 'tp'))
Inputs may be any that keep to these rules, and one draw needn't show every extreme that they name: `query_weight`: entries of order 2048 to the power -1/2. `key_matrix`: entries of order 2048 to the power -1/2.
All inputs are finite; a program needn't handle non-finite values.
Results may differ from a plain program's by a relative error of at most 0.0085.
The roundings to bfloat16 on the way count: a program that leaves them out, or rounds other values in their place, can miss the bound.
Values may be sent and summed in bfloat16 or wider, within the bound.
A program may use at most 128 MiB of HBM per device.

v0:
```python
import math
import jax
import jax.numpy as jnp
from jax import lax
from jax.sharding import PartitionSpec as P

GRID_W = 64
NORM_EPS = 1e-06
ROPE_BASE = 10000.0


def normalize(latent_value_rows):
    return latent_value_rows * lax.rsqrt(
        jnp.mean(latent_value_rows * latent_value_rows, axis=-1, keepdims=True) + NORM_EPS
    )


def rotate(latent_value_rows, positions):
    quarter = latent_value_rows.shape[-1] // 2
    inv_freq = ROPE_BASE ** (-jnp.arange(quarter, dtype=jnp.float32) / quarter)
    angles = positions.astype(jnp.float32)[:, None] * inv_freq[None, :]
    cos_table = jnp.cos(angles)[:, None, :]
    sin_table = jnp.sin(angles)[:, None, :]
    first, second = (latent_value_rows[..., :quarter], latent_value_rows[..., quarter:])
    return jnp.concatenate(
        [first * cos_table - second * sin_table, second * cos_table + first * sin_table], axis=-1
    )


def axial(latent_value_rows, positions):
    half_dim = latent_value_rows.shape[-1] // 2
    return jnp.concatenate(
        [
            rotate(latent_value_rows[..., :half_dim], positions // GRID_W),
            rotate(latent_value_rows[..., half_dim:], positions % GRID_W),
        ],
        axis=-1,
    )


def modulate(latent_value_rows, mod_row):
    model_width = latent_value_rows.shape[-1]
    shift_vec = mod_row[:model_width]
    scale_vec = mod_row[model_width : 2 * model_width]
    return (
        normalize(latent_value_rows.astype(jnp.float32)) * (1.0 + scale_vec) + shift_vec
    ).astype(jnp.bfloat16)


def body(
    latents,
    context,
    cond,
    ctx_cond,
    mod_weight,
    query_weight,
    key_matrix,
    value_matrix,
    out_weight,
    query_gain,
    key_gain,
):
    model_width = latents.shape[1]
    head_dim = query_gain.shape[0]
    sp_count = lax.axis_size("sp")
    partials = jnp.dot(
        jax.nn.silu(jnp.stack([cond, ctx_cond])), mod_weight, precision=lax.Precision.HIGHEST
    )
    summed = lax.psum(partials, "sp")
    modulation = lax.all_gather(summed, "tp", axis=1, tiled=True)
    gate_vec = modulation[0, 2 * model_width :]
    normalised_rows = modulate(latents, modulation[0])
    prefix_normalised = modulate(context, modulation[1])
    query_cols = query_weight.shape[1]
    key_cols = key_matrix.shape[1]
    piece = lax.all_gather(normalised_rows, "tp", axis=0, tiled=True)
    projected = jnp.concatenate(
        [
            jnp.dot(piece, query_weight, preferred_element_type=jnp.float32),
            jnp.dot(piece, key_matrix, preferred_element_type=jnp.float32),
            jnp.dot(piece, value_matrix, preferred_element_type=jnp.float32),
        ],
        axis=1,
    )
    row_count = projected.shape[0]
    positions = lax.axis_index("sp") * row_count + jnp.arange(row_count, dtype=jnp.int32)
    query_heads = projected[:, :query_cols].reshape(row_count, -1, head_dim)
    query_heads = axial(normalize(query_heads) * query_gain, positions).astype(jnp.bfloat16)
    key_heads = projected[:, query_cols : query_cols + key_cols].reshape(row_count, -1, head_dim)
    key_heads = axial(normalize(key_heads) * key_gain, positions).astype(jnp.bfloat16)
    value_heads = (
        projected[:, query_cols + key_cols :].reshape(row_count, -1, head_dim).astype(jnp.bfloat16)
    )
    key_part = jnp.dot(prefix_normalised, key_matrix, preferred_element_type=jnp.float32).reshape(
        prefix_normalised.shape[0], -1, head_dim
    )
    value_part = jnp.dot(
        prefix_normalised, value_matrix, preferred_element_type=jnp.float32
    ).reshape(prefix_normalised.shape[0], -1, head_dim)
    local_keys = (normalize(key_part) * key_gain).astype(jnp.bfloat16)
    local_values = value_part.astype(jnp.bfloat16)
    prefix_keys, prefix_values = (
        lax.all_gather(local_keys, "sp", axis=0, tiled=True),
        lax.all_gather(local_values, "sp", axis=0, tiled=True),
    )
    kv_local = key_heads.shape[1]
    group_size = query_heads.shape[1] // kv_local
    grouped = query_heads.reshape(row_count, kv_local, group_size, head_dim).transpose(1, 2, 0, 3)
    grouped = grouped.reshape(kv_local, group_size * row_count, head_dim)
    inv_root = head_dim ** (-0.5)
    lift = math.log(sp_count * row_count / (2.0 * prefix_keys.shape[0]))
    ctx_scores = (
        jnp.einsum("hqd,khd->hqk", grouped, prefix_keys, preferred_element_type=jnp.float32)
        * inv_root
        + lift
    )
    top_init = jnp.max(ctx_scores, axis=-1)
    ctx_weights = jnp.exp(ctx_scores - top_init[..., None])
    initial = (
        top_init,
        jnp.sum(ctx_weights, axis=-1),
        jnp.einsum(
            "hqk,khd->hqd",
            ctx_weights.astype(jnp.bfloat16),
            prefix_values,
            preferred_element_type=jnp.float32,
        ),
    )

    def update(state_now, key_block, value_block):
        top_old, total_old, acc_old = state_now
        scores = (
            jnp.einsum("hqd,khd->hqk", grouped, key_block, preferred_element_type=jnp.float32)
            * inv_root
        )
        top_new = jnp.maximum(top_old, jnp.max(scores, axis=-1))
        factor = jnp.exp(top_old - top_new)
        weights_now = jnp.exp(scores - top_new[..., None])
        acc_new = acc_old * factor[..., None] + jnp.einsum(
            "hqk,khd->hqd",
            weights_now.astype(jnp.bfloat16),
            value_block,
            preferred_element_type=jnp.float32,
        )
        return (top_new, total_old * factor + jnp.sum(weights_now, axis=-1), acc_new)

    key_piece = lax.all_gather(key_heads, "sp", axis=0, tiled=True)
    value_piece = lax.all_gather(value_heads, "sp", axis=0, tiled=True)
    key_count = key_piece.shape[0]
    rows_per_block = math.gcd(key_count, 2048)
    block_count = key_count // rows_per_block
    key_blocks = key_piece.reshape(block_count, rows_per_block, kv_local, head_dim)
    value_blocks = value_piece.reshape(block_count, rows_per_block, kv_local, head_dim)

    def one_step(state_in, blocks_in):
        return (update(state_in, blocks_in[0], blocks_in[1]), None)

    state_out, _ = lax.scan(one_step, initial, (key_blocks, value_blocks))
    top_fin, total_fin, acc_fin = state_out
    attended = (acc_fin / total_fin[..., None]).astype(jnp.bfloat16)
    attended = (
        attended.reshape(kv_local, group_size, row_count, head_dim)
        .transpose(2, 0, 1, 3)
        .reshape(row_count, -1)
    )
    mixed_rows = lax.psum_scatter(
        jnp.dot(attended, out_weight, preferred_element_type=jnp.float32).astype(jnp.bfloat16),
        "tp",
        scatter_dimension=0,
        tiled=True,
    ).astype(jnp.float32)
    return (latents.astype(jnp.float32) + gate_vec * normalize(mixed_rows)).astype(jnp.bfloat16)


def solution(mesh):
    placed = (
        P(("sp", "tp"), None),
        P("sp", None),
        P("sp"),
        P("sp"),
        P("sp", "tp"),
        P(None, "tp"),
        P(None, "tp"),
        P(None, "tp"),
        P("tp", None),
        P(),
        P(),
    )
    return jax.shard_map(
        body, mesh=mesh, in_specs=placed, out_specs=P(("sp", "tp"), None), check_vma=False
    )
```

profile of v0, /device:TPU:0, one launch (start us, length us, event | category | flops | bytes accessed | tf_op | source)
XLA Modules:
  0.0 286.1 jit_solution(9915169423210026204)
XLA Ops:
  6.5 2.4 fusion.41
  9.0 38.8 %psum.7 = f32[2,1536]{1,0:T(2,128)S(1)} all-reduce(f32[2,1536]{1,0:T(2,128)S(1)} %fusion.41), channel_id=1, replica_groups=mesh['sp'=8,'tp'=4] {'sp'}, use_global_device_ids=true, to_apply=%region_0.1 | all-reduce | flops 3072 | bytes 24576 | tf_op jit(solution)/shard_map/psum | solution.py:69
  47.8 5.2 %all_gather.18 = f32[2,6144]{1,0:T(2,128)S(1)} all-gather(f32[2,1536]{1,0:T(2,128)S(1)} %psum.7), channel_id=1, replica_groups=mesh['sp'=8,'tp'=4] {'tp'}, dimensions={1}, use_global_device_ids=true | all-gather | bytes 61440 | tf_op jit(solution)/shard_map/all_gather | solution.py:70
  53.0 0.6 fusion.55
  53.6 1.2 fusion.27
  54.9 2.1 fusion.30
  56.9 0.0 all-gather.4.cloned.1.call-update
  57.0 0.0 all-gather.6.cloned.1.call-start
  57.1 0.5 multiply_cosine_fusion.1
  57.6 0.1 copy.81
  57.7 0.1 copy.82
  57.9 0.9 copy.83
  58.7 0.9 copy.84
  59.6 17.4 %all-gather.4.cloned.1.call-done = bf16[512,2048]{1,0:T(8,128)(2,1)} async-done(((bf16[128,2048]{1,0:T(8,128)(2,1)}), bf16[512,2048]{1,0:T(8,128)(2,1)}) %all-gather.4.cloned.1.call-update) | async-done | bytes 2097168 | tf_op jit(solution)/shard_map/all_gather | solution.py:76
  77.0 4.0 %multiply_reduce_fusion.1 = (f32[512,2]{0,1:T(2,128)}, f32[512,256]{0,1:T(8,128)}) fusion(bf16[512,2048]{1,0:T(8,128)(2,1)} %all-gather.4.cloned.1.call-done, bf16[2048,256]{1,0:T(8,128)(2,1)} %param.19), kind=kOutput, calls=%fused_computation.57 | convolution fusion | flops 537132032 | bytes 3674112 | tf_op jit(solution)/shard_map/dot_general | solution.py:80
  81.0 1.3 copy.80
  82.3 0.7 add_rsqrt_fusion.1
  83.0 0.9 multiply_multiply_fusion.1
  83.8 1.5 subtract_convert_fusion.1
  85.4 1.1 pad_maximum_fusion.1
  86.5 0.0 all-gather.6.cloned.1.call-update
  86.5 0.0 all-gather.8.cloned.1.call-start
  86.5 0.7 fusion.32
  87.3 3.3 %convolution_convert_fusion.1 = bf16[512,256]{0,1:T(8,128)(2,1)} fusion(bf16[512,2048]{1,0:T(8,128)(2,1)} %all-gather.4.cloned.1.call-done, bf16[2048,256]{1,0:T(8,128)(2,1)} %param.20), kind=kOutput, calls=%fused_computation.32 | convolution fusion | flops 537001984 | bytes 3407872 | tf_op jit(solution)/shard_map/dot_general | solution.py:81
  90.6 1.8 copy.85
  92.4 0.0 all-gather.8.cloned.1.call-update
  92.4 0.0 reduce-scatter.2.cloned.1.call-start
  92.5 0.7 add_rsqrt_fusion.4
  93.1 0.6 copy-done.11
  93.7 1.0 fusion.39
  94.7 0.9 reshape.233
  95.6 0.1 multiply_reduce_fusion.2
  95.7 0.1 copy.76
  95.8 1.6 fusion.24
  97.4 0.9 fusion.37
  98.4 31.6 %all_gather.20 = bf16[512,2,128]{2,0,1:T(8,128)(2,1)S(1)} all-gather(bf16[64,2,128]{2,0,1:T(8,128)(2,1)S(1)} %fusion.37), channel_id=1, replica_groups=mesh['sp'=8,'tp'=4] {'sp'}, dimensions={0}, use_global_device_ids=true | all-gather | bytes 294912 | tf_op jit(solution)/shard_map/all_gather | solution.py:103
  129.9 33.5 %all_gather.21 = bf16[512,2,128]{2,0,1:T(8,128)(2,1)} all-gather(bf16[64,2,128]{2,0,1:T(8,128)(2,1)S(1)} %bitcast.103), channel_id=1, replica_groups=mesh['sp'=8,'tp'=4] {'sp'}, dimensions={0}, use_global_device_ids=true | all-gather | bytes 294912 | tf_op jit(solution)/shard_map/all_gather | solution.py:104
  163.5 3.6 %multiply_reduce_fusion = (f32[512,4]{0,1:T(4,128)S(1)}, f32[512,512]{0,1:T(8,128)S(1)}) fusion(bf16[512,2048]{1,0:T(8,128)(2,1)} %all-gather.4.cloned.1.call-done, bf16[2048,512]{1,0:T(8,128)(2,1)} %param.18), kind=kOutput, calls=%fused_computation.44 | convolution fusion | flops 1074264064 | bytes 5251072 | tf_op jit(solution)/shard_map/dot_general | solution.py:79
  167.1 0.2 multiply_multiply_fusion
  167.3 0.9 subtract_convert_fusion.3
  168.2 0.3 copy.72
  168.5 1.2 copy.73
  169.6 1.9 copy.74
  171.5 1.9 copy.75
  173.5 1.9 pad_maximum_fusion
  175.3 0.8 copy-done.1
  176.1 0.7 fusion.16
  176.9 0.8 fusion.18
  177.7 1.2 fusion.19
  178.9 0.0 all-gather.6.cloned.1.call-done
  179.0 10.1 %all-gather.8.cloned.1.call-done = bf16[4096,2,128]{2,0,1:T(8,128)(2,1)} async-done(((bf16[512,2,128]{2,0,1:T(8,128)(2,1)}), bf16[4096,2,128]{2,0,1:T(8,128)(2,1)}) %all-gather.8.cloned.1.call-update) | async-done | bytes 2097168 | tf_op jit(solution)/shard_map/all_gather | solution.py:148
  189.1 52.1 %while.14 = (s32[]{:T(128)}, f32[2,1024]{1,0:T(2,128)S(1)}, f32[2,1024]{1,0:T(2,128)S(1)}, f32[2,1024,128]{2,1,0:T(8,128)S(1)}, bf16[2,2048,2,128]{3,1,0,2:T(8,1...) while((s32[]{:T(128)}, f32[2,1024]{1,0:T(2,128)S(1)}, ...), condition=%wide.region_11.12_spmd, body=%wide.region_8.11_spmd.sunk | while | flops 2181566464 | bytes 55182420 | solution.py:158
  189.1 9.4 %bitcast_reduce_fusion.2 = (f32[2,1024]{1,0:T(2,128)S(1)}, f32[2,2048,1024]{2,1,0:T(8,128)}) fusion(bf16[2,1024,128]{2,1,0:T(8,128)(2,1)} %get-tuple-element.194, bf16[2,2048,2,128]{3,1,0,2:T(8,128)(2,1)} %get-tuple-element.193, s32[]{:T(128)} %get-tuple-element.181), kind=kOutput, calls=%fused_computation.1.clone.1 | convolution fusion | flops 1082128384 | bytes 18358784 | tf_op jit(solution)/shard_map/while/body/eval_jaxpr/hqd,khd->hqk/dot_general | solution.py:133
  198.5 8.5 %fusion.80 = f32[2,1024]{1,0:T(2,128)S(1)} fusion(f32[2,2048,1024]{2,1,0:T(8,128)} %get-tuple-element.170, f32[2,1024]{1,0:T(2,128)S(1)} %max.4), kind=kLoop, calls=%fused_computation.4.clone.1 | loop fusion | flops 12580864 | bytes 16793600 | tf_op jit(solution)/shard_map/while/body/eval_jaxpr/reduce_sum | solution.py:145
  207.0 8.1 %fusion.81 = f32[2,1024,128]{2,1,0:T(8,128)S(1)} fusion(f32[2,2048,1024]{2,1,0:T(8,128)} %get-tuple-element.170, f32[2,1024]{1,0:T(2,128)S(1)} %max.4, bf16[2,2048,2,128]{3,1,0,2:T(8,128)(2,1)} %get-tuple-element.195, s32[]{:T(128)} %get-tuple-element.181, f32[2,1024,128]{2,1,0:T(8,128)S(1)} %get-tuple-element.184, f32[2,1024]{1,0:T(2,128)S(1)} %get-tuple-element.172), kind=kOutput, calls=%fused_computation.6.clone.1 | convolution fusion | flops 1086849024 | bytes 19939840 | tf_op jit(solution)/shard_map/while/body/eval_jaxpr/hqk,khd->hqd/dot_general | solution.py:139
  215.1 9.4 %bitcast_reduce_fusion.2 = (f32[2,1024]{1,0:T(2,128)S(1)}, f32[2,2048,1024]{2,1,0:T(8,128)}) fusion(bf16[2,1024,128]{2,1,0:T(8,128)(2,1)} %get-tuple-element.194, bf16[2,2048,2,128]{3,1,0,2:T(8,128)(2,1)} %get-tuple-element.193, s32[]{:T(128)} %get-tuple-element.181), kind=kOutput, calls=%fused_computation.1.clone.1 | convolution fusion | flops 1082128384 | bytes 18358784 | tf_op jit(solution)/shard_map/while/body/eval_jaxpr/hqd,khd->hqk/dot_general | solution.py:133
  224.5 8.5 %fusion.80 = f32[2,1024]{1,0:T(2,128)S(1)} fusion(f32[2,2048,1024]{2,1,0:T(8,128)} %get-tuple-element.170, f32[2,1024]{1,0:T(2,128)S(1)} %max.4), kind=kLoop, calls=%fused_computation.4.clone.1 | loop fusion | flops 12580864 | bytes 16793600 | tf_op jit(solution)/shard_map/while/body/eval_jaxpr/reduce_sum | solution.py:145
  233.1 8.1 %fusion.81 = f32[2,1024,128]{2,1,0:T(8,128)S(1)} fusion(f32[2,2048,1024]{2,1,0:T(8,128)} %get-tuple-element.170, f32[2,1024]{1,0:T(2,128)S(1)} %max.4, bf16[2,2048,2,128]{3,1,0,2:T(8,128)(2,1)} %get-tuple-element.195, s32[]{:T(128)} %get-tuple-element.181, f32[2,1024,128]{2,1,0:T(8,128)S(1)} %get-tuple-element.184, f32[2,1024]{1,0:T(2,128)S(1)} %get-tuple-element.172), kind=kOutput, calls=%fused_computation.6.clone.1 | convolution fusion | flops 1086849024 | bytes 19939840 | tf_op jit(solution)/shard_map/while/body/eval_jaxpr/hqk,khd->hqd/dot_general | solution.py:139
  241.2 1.1 divide_convert_fusion
  242.3 1.2 copy.88
  243.6 2.6 convolution_convert_fusion
  246.3 29.9 %reduce-scatter.2.cloned.1.call-done = bf16[128,2048]{1,0:T(8,128)(2,1)} async-done(((bf16[512,2048]{1,0:T(8,128)(2,1)}), bf16[128,2048]{1,0:T(8,128)(2,1)}) %reduce-scatter.2.cloned.1.call-update) | async-done | bytes 524304 | tf_op jit(solution)/shard_map/reduce_scatter | solution.py:166
  276.2 1.2 fusion.25
  277.4 2.1 fusion.31
  (39 shorter events, 0.2 us)
Async XLA Ops:
  6.5 237.1 %copy-start = (bf16[512,2048]{1,0:T(8,128)(2,1)S(1)}, bf16[512,2048]{1,0:T(8,128)(2,1)}, u32[]{:S(2)}) copy-start(bf16[512,2048]{1,0:T(8,128)(2,1)} %param.21) | copy-start | bytes 6291460
  6.5 70.5 %all-gather.4.cloned.1.call-start = ((), (), s32[]{:S(2)}) async-start(), calls=%async_computation.1 | async-start | bytes 2621440 | tf_op jit(solution)/shard_map/all_gather | solution.py:76
  57.0 122.0 %all-gather.6.cloned.1.call-start = ((), (), s32[]{:S(2)}) async-start(), calls=%async_computation.2 | async-start | bytes 2359296 | tf_op jit(solution)/shard_map/all_gather | solution.py:147
  57.6 19.4 %copy-start.6 = (f32[512,32]{0,1:T(8,128)}, f32[512,32]{0,1:T(8,128)S(1)}, u32[]{:S(2)}) copy-start(f32[512,32]{0,1:T(8,128)S(1)} %get-tuple-element.112) | copy-start | bytes 196612
  57.6 19.4 %copy-start.8 = (f32[512,32]{0,1:T(8,128)}, f32[512,32]{0,1:T(8,128)S(1)}, u32[]{:S(2)}) copy-start(f32[512,32]{0,1:T(8,128)S(1)} %get-tuple-element.113) | copy-start | bytes 196612
  81.0 5.5 %copy-start.3 = (bf16[64,2048]{1,0:T(8,128)(2,1)S(1)}, bf16[64,2048]{1,0:T(8,128)(2,1)}, u32[]{:S(2)}) copy-start(bf16[64,2048]{1,0:T(8,128)(2,1)} %param.14) | copy-start | bytes 786436
  85.3 8.4 %copy-start.4 = (bf16[2048,256]{1,0:T(8,128)(2,1)S(1)}, bf16[2048,256]{1,0:T(8,128)(2,1)}, u32[]{:S(2)}) copy-start(bf16[2048,256]{1,0:T(8,128)(2,1)} %param.19) | copy-start | bytes 3145732
  86.5 102.6 %all-gather.8.cloned.1.call-start = ((), (), s32[]{:S(2)}) async-start(), calls=%async_computation.3 | async-start | bytes 2359296 | tf_op jit(solution)/shard_map/all_gather | solution.py:148
  92.4 183.8 %reduce-scatter.2.cloned.1.call-start = ((), (), s32[]{:S(2)}) async-start(), calls=%async_computation.4 | async-start | bytes 2621440 | tf_op jit(solution)/shard_map/reduce_scatter | solution.py:166
  93.1 0.6 copy-start.11
  163.4 3.6 %copy-start.12 = (f32[128]{0:T(128)S(1)}, f32[128]{0:T(128)}, u32[]{:S(2)}) copy-start(f32[128]{0:T(128)} %param.22) | copy-start | bytes 1540
  163.4 3.8 %copy-start.7 = (f32[512,32]{0,1:T(8,128)S(1)}, f32[512,32]{0,1:T(8,128)}, u32[]{:S(2)}) copy-start(f32[512,32]{0,1:T(8,128)} %copy-done.6) | copy-start | bytes 196612
  163.4 3.8 %copy-start.9 = (f32[512,32]{0,1:T(8,128)S(1)}, f32[512,32]{0,1:T(8,128)}, u32[]{:S(2)}) copy-start(f32[512,32]{0,1:T(8,128)} %copy-done.8) | copy-start | bytes 196612
  175.3 0.8 copy-start.1
  176.1 1.6 copy-start.5
  243.6 33.8 %copy-start.2 = (bf16[128,2048]{1,0:T(8,128)(2,1)S(1)}, bf16[128,2048]{1,0:T(8,128)(2,1)}, u32[]{:S(2)}) copy-start(bf16[128,2048]{1,0:T(8,128)(2,1)} %param.13) | copy-start | bytes 1572868
  243.6 33.8 %copy-start.10 = (f32[1,2048]{1,0:T(1,128)S(1)}, f32[1,2048]{1,0:T(1,128)}, u32[]{:S(2)}) copy-start(f32[1,2048]{1,0:T(1,128)} %get-tuple-element.103) | copy-start | bytes 24580
Sparse Core Ops, SparseCore 0:
  57.1 19.8 all-gather.3
  86.6 52.3 all-gather.5
  141.2 47.7 all-gather.7
  246.4 29.7 reduce-scatter.1
where the time goes:
time: 287 us; the launch traced here: 286 us
  blocking collectives  109 us (38%)
  waiting for transfers between devices  57.5 us (20%)
  matrix products  55.5 us (19%)
  other arithmetic  36.5 us (13%)
  local copies, waits for them, and re-layouts  13.9 us (5%)
  between operations  13.4 us (5%)
    psum x1, blocking collectives, body(): summed = lax.psum(partials, 'sp')  38.8 us
    all_gather x1, blocking collectives, body(): lax.all_gather(local_values, 'sp', axis=0, tiled=True)  33.5 us
    all_gather x1, blocking collectives, body(): lax.all_gather(local_keys, 'sp', axis=0, tiled=True)  31.6 us
    reduce_scatter x1, waiting for transfers between devices, body(): lax.psum_scatter(jnp.dot(attended, out_weight, preferred_element_type=jnp...  29.9 us
    dot_general x2, matrix products, update(): jnp.einsum('hqd,khd->hqk', grouped, key_block, preferred_element_type=jnp...  18.8 us
    all_gather x1, waiting for transfers between devices, body(): piece = lax.all_gather(normalised_rows, 'tp', axis=0, tiled=True)  17.4 us
    reduce_sum x2, other arithmetic, update(): jnp.sum(weights_now, axis=-1)  17 us
    dot_general x2, matrix products, update(): jnp.einsum('hqk,khd->hqd', weights_now.astype(jnp.bfloat16), value_block,...  16.2 us
  transfers between devices with their start and end apart: 4, of which 3 were waited for; matrix products, arithmetic and copies ran while one was open for 10% of the time, Pallas kernels for 0%

commit v1 on v0

--- a/solution.py
+++ b/solution.py
@@ -73,7 +73,10 @@
     prefix_normalised = modulate(context, modulation[1])
     query_cols = query_weight.shape[1]
     key_cols = key_matrix.shape[1]
-    piece = lax.all_gather(normalised_rows, "tp", axis=0, tiled=True)
+    devices = lax.axis_size("tp")
+    pieces = jnp.stack([normalised_rows for _ in range(devices)])
+    pieces = lax.all_to_all(pieces, "tp", split_axis=0, concat_axis=0)
+    piece = jnp.concatenate(pieces, axis=0)
     projected = jnp.concatenate(
         [
             jnp.dot(piece, query_weight, preferred_element_type=jnp.float32),

time: 287 us -> 290 us (1.010)
  local copies, waits for them, and re-layouts: 13.9 us -> 22.6 us
  waiting for transfers between devices: 57.5 us -> 52.2 us
  other arithmetic: 36.5 us -> 31.6 us
  starting transfers between devices: 0.13 us -> 4.57 us
    all_to_all x0 -> x1, waiting for transfers between devices: none -> 23 us  [body(): pieces = lax.all_to_all(pieces, 'tp', split_axis=0, concat_axis=0)]
    all_gather x1 -> x0, waiting for transfers between devices: 17.4 us -> none  [body(): piece = lax.all_gather(normalised_rows, 'tp', axis=0, tiled=True)]
    all_gather x1, waiting for transfers between devices: 10.1 us -> 0.01 us  [body(): value_piece = lax.all_gather(value_heads, 'sp', axis=0, tiled=True)]
    dot_general x0 -> x3, local copies, waits for them, and re-layouts: none -> 7.68 us  [the longest x1 3.94 us: body(): jnp.dot(piece, query_weight, preferred_element_type=jnp.float32)]
    while x2 -> x3, local copies, waits for them, and re-layouts: 0.01 us -> 6.18 us  [the longest x1 6.17 us: body(): state_out, _ = lax.scan(one_step, initial, (key_blocks, value_blocks))]
    concatenate x4 -> x0, local copies, waits for them, and re-layouts: 5.26 us -> none  [axial(): jnp.concatenate([rotate(latent_value_rows[..., :half_dim], positions // G...]
    all_to_all x0 -> x1, starting transfers between devices: none -> 4.44 us  [body(): pieces = lax.all_to_all(pieces, 'tp', split_axis=0, concat_axis=0)]
    reshape x1, local copies, waits for them, and re-layouts: 1.27 us -> 4.67 us  [body(): key_piece.reshape(block_count, rows_per_block, kv_local, head_dim)]
  transfers between devices with their start and end apart: 4 -> 4, of which waited for: 3 -> 2; matrix products, arithmetic and copies ran while one was open for 10% -> 13% of each run, Pallas kernels for 0% -> 0%
where the time goes in v1:
time: 290 us; the launch traced here: 289 us
  blocking collectives  110 us (38%)
  matrix products  54.8 us (19%)
  waiting for transfers between devices  52.2 us (18%)
  other arithmetic  31.6 us (11%)
  local copies, waits for them, and re-layouts  22.6 us (8%)
  between operations  13.4 us (5%)
  starting transfers between devices  4.57 us (2%)
    psum x1, blocking collectives, body(): summed = lax.psum(partials, 'sp')  38.8 us
    all_gather x1, blocking collectives, body(): lax.all_gather(local_values, 'sp', axis=0, tiled=True)  33.4 us
    all_gather x1, blocking collectives, body(): lax.all_gather(local_keys, 'sp', axis=0, tiled=True)  32.3 us
    reduce_scatter x1, waiting for transfers between devices, body(): lax.psum_scatter(jnp.dot(attended, out_weight, preferred_element_type=jnp...  29.1 us
    all_to_all x1, waiting for transfers between devices, body(): pieces = lax.all_to_all(pieces, 'tp', split_axis=0, concat_axis=0)  23 us
    dot_general x2, matrix products, update(): jnp.einsum('hqd,khd->hqk', grouped, key_block, preferred_element_type=jnp...  18.8 us
    reduce_sum x2, other arithmetic, update(): jnp.sum(weights_now, axis=-1)  17 us
    dot_general x2, matrix products, update(): jnp.einsum('hqk,khd->hqd', weights_now.astype(jnp.bfloat16), value_block,...  16.2 us
  transfers between devices with their start and end apart: 4, of which 2 were waited for; matrix products, arithmetic and copies ran while one was open for 13% of the time, Pallas kernels for 0%

profile of v1, /device:TPU:0, one launch (start us, length us, event | category | flops | bytes accessed | tf_op | source)
XLA Modules:
  0.0 289.0 jit_solution(6575570806211687196)
XLA Ops:
  6.5 0.0 copy-start
  6.5 2.4 fusion.41
  9.0 38.8 %psum.7 = f32[2,1536]{1,0:T(2,128)S(1)} all-reduce(f32[2,1536]{1,0:T(2,128)S(1)} %fusion.41), channel_id=1, replica_groups=mesh['sp'=8,'tp'=4] {'sp'}, use_global_device_ids=true, to_apply=%region_0.1 | all-reduce | flops 3072 | bytes 24576 | tf_op jit(solution)/shard_map/psum | solution.py:69
  47.8 5.2 %all_gather.15 = f32[2,6144]{1,0:T(2,128)S(1)} all-gather(f32[2,1536]{1,0:T(2,128)S(1)} %psum.7), channel_id=1, replica_groups=mesh['sp'=8,'tp'=4] {'tp'}, dimensions={1}, use_global_device_ids=true | all-gather | bytes 61440 | tf_op jit(solution)/shard_map/all_gather | solution.py:70
  53.0 0.6 fusion.55
  53.6 1.3 fusion.27
  55.0 1.3 fusion.30
  56.2 1.6 stack.19
  57.8 4.4 %all-to-all-start = ((bf16[4,128,2048]{2,1,0:T(8,128)(2,1)}), bf16[4,128,2048]{2,1,0:T(8,128)(2,1)}, u32[]{:S(2)}, u32[]{:S(2)}) async-start(bf16[4,128,2048]{2,1,0:T(8,128)(2,1)} %stack.19), calls=%async_computation | async-start | bytes 4194304 | tf_op jit(solution)/shard_map/all_to_all | solution.py:78
  62.2 0.0 all-gather.3.cloned.1.call-start
  62.3 0.0 copy-done.3
  62.3 1.4 copy.70
  63.8 1.2 multiply_cosine_fusion.1
  65.0 23.0 %all-to-all-done = bf16[4,128,2048]{2,1,0:T(8,128)(2,1)} async-done(((bf16[4,128,2048]{2,1,0:T(8,128)(2,1)}), bf16[4,128,2048]{2,1,0:T(8,128)(2,1)}, u32[]{:S(2)}, u32[]{:S(2)}) %all-to-all-start) | async-done | bytes 2097184 | tf_op jit(solution)/shard_map/all_to_all | solution.py:78
  88.0 2.7 multiply_reduce_fusion.1
  90.7 0.8 multiply_multiply_fusion.1
  91.5 0.1 subtract_convert_fusion.3
  91.6 0.7 pad_maximum_fusion
  92.3 0.0 all-gather.3.cloned.1.call-update
  92.3 0.0 all-gather.5.cloned.1.call-start
  92.4 2.3 copy.71
  94.6 0.7 fusion.32
  95.3 3.4 %convolution_convert_fusion.1 = bf16[512,2,128]{2,0,1:T(8,128)(2,1)} fusion(bf16[512,2048,1]{1,0,2:T(8,128)(2,1)} %bitcast.9, bf16[2,128,2048]{2,1,0:T(8,128)(2,1)} %bitcast.102), kind=kOutput, calls=%fused_computation.32 | convolution fusion | flops 537001984 | bytes 3407872 | tf_op jit(solution)/shard_map/dot_general | solution.py:84
  98.7 0.0 all-gather.5.cloned.1.call-update
  98.7 0.0 reduce-scatter.2.cloned.1.call-start
  98.8 1.1 add_rsqrt_fusion.4
  99.9 3.9 %copy.69 = bf16[512,2048]{1,0:T(8,128)(2,1)} copy(bf16[512,2048]{0,1:T(8,128)(2,1)} %bitcast.99) | data formatting | bytes 4194304 | tf_op jit(solution)/shard_map/dot_general | solution.py:82
  103.8 1.6 fusion.39
  105.4 0.9 reshape.236
  106.3 0.1 multiply_reduce_fusion.2
  106.4 0.1 copy.58
  106.5 1.6 fusion.24
  108.1 0.9 fusion.37
  109.0 32.3 %all_gather.16 = bf16[512,2,128]{2,0,1:T(8,128)(2,1)S(1)} all-gather(bf16[64,2,128]{2,0,1:T(8,128)(2,1)S(1)} %fusion.37), channel_id=1, replica_groups=mesh['sp'=8,'tp'=4] {'sp'}, dimensions={0}, use_global_device_ids=true | all-gather | bytes 294912 | tf_op jit(solution)/shard_map/all_gather | solution.py:106
  141.3 33.4 %all_gather.17 = bf16[512,2,128]{2,0,1:T(8,128)(2,1)} all-gather(bf16[64,2,128]{2,0,1:T(8,128)(2,1)S(1)} %bitcast.108), channel_id=1, replica_groups=mesh['sp'=8,'tp'=4] {'sp'}, dimensions={0}, use_global_device_ids=true | all-gather | bytes 294912 | tf_op jit(solution)/shard_map/all_gather | solution.py:107
  174.7 3.6 %multiply_reduce_fusion = (f32[512,4]{0,1:T(4,128)S(1)}, f32[512,4,128]{0,2,1:T(8,128)S(1)}) fusion(bf16[512,2048,1]{1,0,2:T(8,128)(2,1)} %bitcast.9, bf16[4,128,2048]{2,1,0:T(8,128)(2,1)} %bitcast.100), kind=kOutput, calls=%fused_computation.44 | convolution fusion | flops 1074264064 | bytes 5251072 | tf_op jit(solution)/shard_map/dot_general | solution.py:82
  178.3 0.2 multiply_multiply_fusion
  178.5 0.2 subtract_convert_fusion.1
  178.7 0.3 copy.57
  179.0 0.0 copy-start.1
  179.0 0.0 copy-start.5
  179.0 0.7 fusion.16
  179.8 0.1 copy-done.1
  179.8 0.8 fusion.18
  180.7 1.2 fusion.19
  181.9 0.0 all-gather.3.cloned.1.call-done
  181.9 4.7 %reshape.237 = bf16[2,2048,2,128]{1,0,3,2:T(2,128)(2,1)} reshape(bf16[4096,2,128]{0,2,1:T(8,128)(2,1)} %all-gather.3.cloned.1.call-done) | data formatting | bytes 4194304 | tf_op jit(solution)/shard_map/reshape | solution.py:155
  186.6 6.2 %copy.64 = bf16[2,2048,2,128]{3,1,2,0:T(8,128)(2,1)} copy(bf16[2,2048,2,128]{1,0,3,2:T(2,128)(2,1)} %reshape.237) | data formatting | bytes 4194304 | tf_op jit(solution)/shard_map/while | solution.py:161
  192.8 52.1 %while.14 = (s32[]{:T(128)}, f32[2,1024]{1,0:T(2,128)S(1)}, f32[2,1024]{1,0:T(2,128)S(1)}, f32[2,1024,128]{2,1,0:T(8,128)S(1)}, bf16[2,2048,2,128]{3,1,2,0:T(8,1...) while((s32[]{:T(128)}, f32[2,1024]{1,0:T(2,128)S(1)}, ...), condition=%wide.region_11.12_spmd, body=%wide.region_8.11_spmd.sunk | while | flops 2181566464 | bytes 55182420 | solution.py:161
  192.8 9.4 %bitcast_reduce_fusion.2 = (f32[2,1024]{1,0:T(2,128)S(1)}, f32[2,2048,1024]{2,1,0:T(8,128)}) fusion(bf16[2,1024,128]{2,1,0:T(8,128)(2,1)} %get-tuple-element.201, bf16[2,2048,2,128]{3,1,2,0:T(8,128)(2,1)} %get-tuple-element.200, s32[]{:T(128)} %get-tuple-element.188), kind=kOutput, calls=%fused_computation.1.clone.1 | convolution fusion | flops 1082128384 | bytes 18358784 | tf_op jit(solution)/shard_map/while/body/eval_jaxpr/hqd,khd->hqk/dot_general | solution.py:136
  202.2 8.5 %fusion.80 = f32[2,1024]{1,0:T(2,128)S(1)} fusion(f32[2,2048,1024]{2,1,0:T(8,128)} %get-tuple-element.177, f32[2,1024]{1,0:T(2,128)S(1)} %max.4), kind=kLoop, calls=%fused_computation.4.clone.1 | loop fusion | flops 12580864 | bytes 16793600 | tf_op jit(solution)/shard_map/while/body/eval_jaxpr/reduce_sum | solution.py:148
  210.7 8.1 %fusion.81 = f32[2,1024,128]{2,1,0:T(8,128)S(1)} fusion(f32[2,2048,1024]{2,1,0:T(8,128)} %get-tuple-element.177, f32[2,1024]{1,0:T(2,128)S(1)} %max.4, bf16[2,2048,2,128]{3,1,0,2:T(8,128)(2,1)} %get-tuple-element.202, s32[]{:T(128)} %get-tuple-element.188, f32[2,1024,128]{2,1,0:T(8,128)S(1)} %get-tuple-element.191, f32[2,1024]{1,0:T(2,128)S(1)} %get-tuple-element.179), kind=kOutput, calls=%fused_computation.6.clone.1 | convolution fusion | flops 1086849024 | bytes 19939840 | tf_op jit(solution)/shard_map/while/body/eval_jaxpr/hqk,khd->hqd/dot_general | solution.py:142
  218.9 9.4 %bitcast_reduce_fusion.2 = (f32[2,1024]{1,0:T(2,128)S(1)}, f32[2,2048,1024]{2,1,0:T(8,128)}) fusion(bf16[2,1024,128]{2,1,0:T(8,128)(2,1)} %get-tuple-element.201, bf16[2,2048,2,128]{3,1,2,0:T(8,128)(2,1)} %get-tuple-element.200, s32[]{:T(128)} %get-tuple-element.188), kind=kOutput, calls=%fused_computation.1.clone.1 | convolution fusion | flops 1082128384 | bytes 18358784 | tf_op jit(solution)/shard_map/while/body/eval_jaxpr/hqd,khd->hqk/dot_general | solution.py:136
  228.3 8.5 %fusion.80 = f32[2,1024]{1,0:T(2,128)S(1)} fusion(f32[2,2048,1024]{2,1,0:T(8,128)} %get-tuple-element.177, f32[2,1024]{1,0:T(2,128)S(1)} %max.4), kind=kLoop, calls=%fused_computation.4.clone.1 | loop fusion | flops 12580864 | bytes 16793600 | tf_op jit(solution)/shard_map/while/body/eval_jaxpr/reduce_sum | solution.py:148
  236.8 8.1 %fusion.81 = f32[2,1024,128]{2,1,0:T(8,128)S(1)} fusion(f32[2,2048,1024]{2,1,0:T(8,128)} %get-tuple-element.177, f32[2,1024]{1,0:T(2,128)S(1)} %max.4, bf16[2,2048,2,128]{3,1,0,2:T(8,128)(2,1)} %get-tuple-element.202, s32[]{:T(128)} %get-tuple-element.188, f32[2,1024,128]{2,1,0:T(8,128)S(1)} %get-tuple-element.191, f32[2,1024]{1,0:T(2,128)S(1)} %get-tuple-element.179), kind=kOutput, calls=%fused_computation.6.clone.1 | convolution fusion | flops 1086849024 | bytes 19939840 | tf_op jit(solution)/shard_map/while/body/eval_jaxpr/hqk,khd->hqd/dot_general | solution.py:142
  244.9 1.1 divide_convert_fusion
  246.1 1.2 copy.66
  247.3 0.0 copy-done
  247.3 0.0 copy-start.2
  247.3 2.6 convolution_convert_fusion
  250.0 0.0 reduce-scatter.2.cloned.1.call-update
  250.0 29.1 %reduce-scatter.2.cloned.1.call-done = bf16[128,2048]{1,0:T(8,128)(2,1)} async-done(((bf16[512,2048]{1,0:T(8,128)(2,1)}), bf16[128,2048]{1,0:T(8,128)(2,1)}) %reduce-scatter.2.cloned.1.call-update) | async-done | bytes 524304 | tf_op jit(solution)/shard_map/reduce_scatter | solution.py:169
  279.1 1.2 fusion.25
  280.3 2.1 fusion.31
  (33 shorter events, 0.2 us)
Async XLA Ops:
  6.5 240.8 %copy-start = (bf16[512,2048]{1,0:T(8,128)(2,1)S(1)}, bf16[512,2048]{1,0:T(8,128)(2,1)}, u32[]{:S(2)}) copy-start(bf16[512,2048]{1,0:T(8,128)(2,1)} %param.21) | copy-start | bytes 6291460
  53.6 8.7 %copy-start.3 = (bf16[2048,256]{1,0:T(8,128)(2,1)S(1)}, bf16[2048,256]{1,0:T(8,128)(2,1)}, u32[]{:S(2)}) copy-start(bf16[2048,256]{1,0:T(8,128)(2,1)} %param.19) | copy-start | bytes 3145732
  57.8 30.2 %all-to-all-start = ((bf16[4,128,2048]{2,1,0:T(8,128)(2,1)}), bf16[4,128,2048]{2,1,0:T(8,128)(2,1)}, u32[]{:S(2)}, u32[]{:S(2)}) async-start(bf16[4,128,2048]{2,1,0:T(8,128)(2,1)} %stack.19), calls=%async_computation | async-start | bytes 4194304 | tf_op jit(solution)/shard_map/all_to_all | solution.py:78
  62.2 119.7 %all-gather.3.cloned.1.call-start = ((), (), s32[]{:S(2)}) async-start(), calls=%async_computation.2 | async-start | bytes 2359296 | tf_op jit(solution)/shard_map/all_gather | solution.py:150
  88.0 3.5 %copy-start.6 = (f32[512,32]{0,1:T(8,128)S(1)}, f32[512,32]{0,1:T(8,128)}, u32[]{:S(2)}) copy-start(f32[512,32]{0,1:T(8,128)} %get-tuple-element.119) | copy-start | bytes 196612
  88.0 3.5 %copy-start.8 = (f32[512,32]{0,1:T(8,128)S(1)}, f32[512,32]{0,1:T(8,128)}, u32[]{:S(2)}) copy-start(f32[512,32]{0,1:T(8,128)} %get-tuple-element.120) | copy-start | bytes 196612
  88.0 6.7 %copy-start.4 = (bf16[64,2048]{1,0:T(8,128)(2,1)S(1)}, bf16[64,2048]{1,0:T(8,128)(2,1)}, u32[]{:S(2)}) copy-start(bf16[64,2048]{1,0:T(8,128)(2,1)} %param.14) | copy-start | bytes 786436
  92.3 100.5 %all-gather.5.cloned.1.call-start = ((), (), s32[]{:S(2)}) async-start(), calls=%async_computation.3 | async-start | bytes 2359296 | tf_op jit(solution)/shard_map/all_gather | solution.py:151
  98.7 180.4 %reduce-scatter.2.cloned.1.call-start = ((), (), s32[]{:S(2)}) async-start(), calls=%async_computation.4 | async-start | bytes 2621440 | tf_op jit(solution)/shard_map/reduce_scatter | solution.py:169
  141.3 37.0 %copy-start.11 = (f32[128]{0:T(128)S(1)}, f32[128]{0:T(128)}, u32[]{:S(2)}) copy-start(f32[128]{0:T(128)} %param.22) | copy-start | bytes 1540
  174.7 3.8 %copy-start.7 = (f32[512,32]{0,1:T(8,128)S(1)}, f32[512,32]{0,1:T(8,128)}, u32[]{:S(2)}) copy-start(f32[512,32]{0,1:T(8,128)} %get-tuple-element.119) | copy-start | bytes 196612
  174.7 3.8 %copy-start.9 = (f32[512,32]{0,1:T(8,128)S(1)}, f32[512,32]{0,1:T(8,128)}, u32[]{:S(2)}) copy-start(f32[512,32]{0,1:T(8,128)} %get-tuple-element.120) | copy-start | bytes 196612
  179.0 0.8 copy-start.1
  179.0 1.6 copy-start.5
  247.3 33.0 %copy-start.2 = (bf16[128,2048]{1,0:T(8,128)(2,1)S(1)}, bf16[128,2048]{1,0:T(8,128)(2,1)}, u32[]{:S(2)}) copy-start(bf16[128,2048]{1,0:T(8,128)(2,1)} %param.13) | copy-start | bytes 1572868
  247.3 33.0 %copy-start.10 = (f32[1,2048]{1,0:T(1,128)S(1)}, f32[1,2048]{1,0:T(1,128)}, u32[]{:S(2)}) copy-start(f32[1,2048]{1,0:T(1,128)} %get-tuple-element.110) | copy-start | bytes 24580
Sparse Core Ops, SparseCore 0:
  92.4 49.3 all-gather.2
  144.0 47.9 all-gather.4
  250.1 28.9 reduce-scatter.1
